TPU v7x, 32 devices: a whole 2x2x4 slice. The times are simulated.
32 devices in a mesh: grp: 2 (over y), sp: 4 (over z), tp: 4 (over x, core).
Axes of the slice: x: 2, y: 2, z: 4, core: 2. Of those that a mesh axis runs over, the one named last changes fastest.
Arguments:
- residual: bfloat16 [2048, 2048], P(('grp', 'sp')), parts along dimension 0, may hold values from -6 to 6
- queries: bfloat16 [2048, 1024], P(('grp', 'sp'), 'tp'), parts along dimension 0, may hold values from -400 to 400
- keys: bfloat16 [2048, 1024], P(('grp', 'sp'), 'tp'), parts along dimension 0, may hold values from -8 to 8
- values: bfloat16 [2048, 1024], P(('grp', 'sp'), 'tp'), parts along dimension 0, may hold values from -6 to 6
- log_gates: float32 [2048, 16], P(('grp', 'sp'), 'tp'), parts along dimension 0, may hold values from -126 to 0, as said below
- w_out: bfloat16 [1024, 2048], P('tp'), may hold values from -0.75 to 0.75
- norm_gain: float32 [2048], replicated, may hold values from 0.1 to 1.9
- w_gate: bfloat16 [2048, 5632], P('sp', 'tp'), may hold values from -0.125 to 0.125
- w_up: bfloat16 [2048, 5632], P('sp', 'tp'), may hold values from -0.125 to 0.125
- w_down: bfloat16 [5632, 2048], P('tp', 'sp'), may hold values from -0.078125 to 0.078125
Outputs:
- output: bfloat16 [2048, 2048], P(('grp', 'sp', 'tp')), parts along dimension 0
There are 2 independent parts, one for each index of `grp`. A program takes and returns all parts, laid end to end along the dimension named above; an argument that names none is the same for every part. Nothing has to cross between parts.
Inputs may be any that keep to these rules, and one draw needn't show every extreme that they name: `log_gates`: never rises along positions.
All inputs are finite; a program needn't handle non-finite values.
Results may differ from a plain program's by a relative error of at most 0.014.
Values may be sent and summed in bfloat16 or wider, within the bound.
A program may use at most 128 MiB of HBM per device.

v0:
```python
import math
import jax
import jax.numpy as jnp
from jax import lax
from jax.sharding import PartitionSpec as P


def normalize(rows_in, gain):
    floats = rows_in.astype(jnp.float32)
    scaled = floats * lax.rsqrt(jnp.mean(floats * floats, axis=-1, keepdims=True) + 1e-06)
    return (scaled * gain).astype(jnp.bfloat16)


def attend(queries, keys, values, log_gates):
    row_count = queries.shape[0]
    head_count = log_gates.shape[1]
    head_width = queries.shape[1] // head_count
    score_scale = head_width ** (-0.5)
    first_row = lax.axis_index("sp") * row_count
    query_heads = queries.reshape(row_count, head_count, head_width)
    query_gates = log_gates.T
    query_positions = first_row + jnp.arange(row_count, dtype=jnp.int32)
    initial = (
        jnp.full((head_count, row_count), -1e30, jnp.float32),
        jnp.zeros((head_count, row_count), jnp.float32),
        jnp.zeros((head_count, row_count, head_width), jnp.float32),
    )
    carried = initial
    key_piece = lax.all_gather(keys.astype(jnp.float32), "sp", axis=0, tiled=True).astype(
        jnp.bfloat16
    )
    value_piece = lax.all_gather(values.astype(jnp.float32), "sp", axis=0, tiled=True).astype(
        jnp.bfloat16
    )
    gate_piece = lax.all_gather(log_gates, "sp", axis=0, tiled=True)
    length = key_piece.shape[0]
    block_rows = math.gcd(length, 2048)
    block_count = length // block_rows
    key_blocks = key_piece.reshape(block_count, block_rows, head_count, head_width)
    value_blocks = value_piece.reshape(block_count, block_rows, head_count, head_width)
    gate_blocks = gate_piece.reshape(block_count, block_rows, head_count)
    offsets = jnp.arange(block_count, dtype=jnp.int32) * block_rows

    def one_block(state, inputs):
        current_key_block, value_block, gate_block, offset = inputs

        def work(current):
            running_max, running_sum, accumulated = current
            scores = (
                jnp.einsum(
                    "qhd,khd->hqk",
                    query_heads,
                    current_key_block,
                    preferred_element_type=jnp.float32,
                )
                * score_scale
            )
            scores = scores + query_gates[:, :, None] - gate_block.T[:, None, :]
            key_positions = offset + jnp.arange(block_rows, dtype=jnp.int32)
            causal = (query_positions[:, None] >= key_positions[None, :])[None]
            scores = jnp.where(causal, scores, -1e30)
            new_max = jnp.maximum(running_max, jnp.max(scores, axis=-1))
            weights = jnp.where(causal, jnp.exp(scores - new_max[:, :, None]), 0.0)
            rescale = jnp.exp(running_max - new_max)
            running_sum = running_sum * rescale + jnp.sum(weights, axis=-1)
            product = jnp.einsum(
                "hqk,khd->hqd",
                weights.astype(jnp.bfloat16),
                value_block,
                preferred_element_type=jnp.float32,
            )
            accumulated = accumulated * rescale[:, :, None] + product
            return (new_max, running_sum, accumulated)

        state = lax.cond(offset <= first_row + row_count - 1, work, lambda current: current, state)
        return (state, None)

    carried, _ = lax.scan(one_block, carried, (key_blocks, value_blocks, gate_blocks, offsets))
    running_max, running_sum, accumulated = carried
    attended = accumulated / running_sum[:, :, None]
    return (
        attended.transpose(1, 0, 2).reshape(row_count, head_count * head_width).astype(jnp.bfloat16)
    )


def body(residual, queries, keys, values, log_gates, w_out, norm_gain, w_gate, w_up, w_down):
    attended = attend(queries, keys, values, log_gates)
    row_count = attended.shape[0]
    per_device = row_count // lax.axis_size("tp")
    my_first = lax.axis_index("tp") * per_device
    projected = lax.psum(
        jnp.dot(attended, w_out, preferred_element_type=jnp.float32).astype(jnp.bfloat16), "tp"
    ).astype(jnp.float32)
    mixed_all = (residual.astype(jnp.float32) + projected).astype(jnp.bfloat16)
    normed_all = normalize(mixed_all, norm_gain)
    mixed = lax.dynamic_slice_in_dim(mixed_all, my_first, per_device, 0)
    gate_whole = lax.all_gather(w_gate, "sp", axis=0, tiled=True)
    up_whole = lax.all_gather(w_up, "sp", axis=0, tiled=True)
    down_whole = lax.all_gather(w_down, "sp", axis=1, tiled=True)
    gate_proj = jnp.dot(normed_all, gate_whole, preferred_element_type=jnp.float32)
    up_proj = jnp.dot(normed_all, up_whole, preferred_element_type=jnp.float32)
    hidden = (jax.nn.silu(gate_proj) * up_proj).astype(jnp.bfloat16)
    down_sum = lax.psum_scatter(
        jnp.dot(hidden, down_whole, preferred_element_type=jnp.float32).astype(jnp.bfloat16),
        "tp",
        scatter_dimension=0,
        tiled=True,
    ).astype(jnp.float32)
    summed = mixed.astype(jnp.float32) + 0.5 * down_sum
    scaled = summed * lax.rsqrt(jnp.mean(summed * summed, axis=-1, keepdims=True) + 1e-06)
    return scaled.astype(jnp.bfloat16)


def solution(mesh):
    in_specs = (
        P(("grp", "sp"), None),
        P(("grp", "sp"), "tp"),
        P(("grp", "sp"), "tp"),
        P(("grp", "sp"), "tp"),
        P(("grp", "sp"), "tp"),
        P("tp", None),
        P(),
        P("sp", "tp"),
        P("sp", "tp"),
        P("tp", "sp"),
    )
    out_specs = P(("grp", "sp", "tp"), None)
    return jax.shard_map(body, mesh=mesh, in_specs=in_specs, out_specs=out_specs, check_vma=False)
```

profile of v0, /device:TPU:0, one launch (start us, length us, event | category | flops | bytes accessed | tf_op | source)
XLA Modules:
  0.0 429.7 jit_solution(2206887288210929115)
XLA Ops:
  7.4 1.1 copy.12
  8.5 17.4 %all_gather.18 = bf16[1024,256]{0,1:T(8,128)(2,1)S(1)} all-gather(bf16[256,256]{0,1:T(8,128)(2,1)S(1)} %copy.12), channel_id=1, replica_groups=mesh['grp'=2,'sp'=4,'tp'=4] {'sp'}, dimensions={0}, use_global_device_ids=true | all-gather | bytes 655360 | tf_op jit(solution)/shard_map/all_gather | solution.py:29
  25.8 1.0 copy.13
  26.9 16.3 %all_gather.20 = bf16[1024,256]{0,1:T(8,128)(2,1)S(1)} all-gather(bf16[256,256]{0,1:T(8,128)(2,1)S(1)} %copy.13), channel_id=1, replica_groups=mesh['grp'=2,'sp'=4,'tp'=4] {'sp'}, dimensions={0}, use_global_device_ids=true | all-gather | bytes 655360 | tf_op jit(solution)/shard_map/all_gather | solution.py:32
  43.1 13.3 %all_gather.19 = f32[1024,4]{0,1:T(4,128)S(1)} all-gather(f32[256,4]{0,1:T(4,128)} %param.16), channel_id=1, replica_groups=mesh['grp'=2,'sp'=4,'tp'=4] {'sp'}, dimensions={0}, use_global_device_ids=true | all-gather | bytes 20480 | tf_op jit(solution)/shard_map/all_gather | solution.py:35
  56.5 7.0 %conditional.1 = ((f32[4,256]{1,0:T(4,128)S(1)}, f32[4,256,64]{1,2,0:T(8,128)S(1)})) conditional(s32[]{:T(128)} %convert_element_type.64, (f32[4,256]{1,0:T(4,128)S(1)}, f32[4,256,64]{1,2,0:T(8,128)S(1)}) %tuple.22, (s32[]{:T(128)}, s32[256]{0:T(256)S(1)}, bf16[256,256]{1,0:T(8,128)(2,1)}, bf16[1024,256]{0,1:T(8,128)(2,1)S(1)}, f32[4,256]{1,0:T(4,128)}, ...), branch_computations={%region_0.1_spmd, %region_1.0_spmd} | conditional | flops 288754944 | bytes 15727672 | solution.py:75
  56.8 1.0 copy.14
  57.8 2.1 fusion.2
  59.9 2.0 fusion.1
  61.9 1.6 fusion.6
  63.6 1.4 convolution_convert_fusion
  65.1 0.5 all-gather.4.cloned.1.call-update
  65.7 0.5 all-gather.6.cloned.1.call-update
  66.3 0.5 all-gather.8.cloned.1.call-update
  66.8 35.4 %all-reduce.2.cloned.1.call-done = bf16[256,2048]{1,0:T(8,128)(2,1)} async-done(((bf16[256,2048]{1,0:T(8,128)(2,1)}), bf16[256,2048]{1,0:T(8,128)(2,1)}) %all-reduce.2.cloned.1.call-update) | async-done | bytes 1048592 | tf_op jit(solution)/shard_map/psum | solution.py:91
  102.2 1.7 fusion.13
  104.0 70.1 %all-gather.4.cloned.1.call-done = bf16[2048,1408]{1,0:T(8,128)(2,1)} async-done(((bf16[512,1408]{1,0:T(8,128)(2,1)}), bf16[2048,1408]{1,0:T(8,128)(2,1)}) %all-gather.4.cloned.1.call-update) | async-done | bytes 5767184 | tf_op jit(solution)/shard_map/all_gather | solution.py:97
  174.1 5.6 %fusion.18 = f32[256,1408]{1,0:T(8,128)} fusion(bf16[2048,1408]{1,0:T(8,128)(2,1)} %all-gather.4.cloned.1.call-done, bf16[256,2048]{1,0:T(8,128)(2,1)S(1)} %get-tuple-element.132, f32[2048]{0:T(1024)S(1)} %copy-done.3, f32[256]{0:T(256)S(1)} %add_rsqrt_fusion), kind=kOutput, calls=%fused_computation.29 | convolution fusion | flops 1478492160 | bytes 8266752 | tf_op jit(solution)/shard_map/dot_general | solution.py:100
  179.8 100.6 %all-gather.6.cloned.1.call-done = bf16[2048,1408]{1,0:T(8,128)(2,1)} async-done(((bf16[512,1408]{1,0:T(8,128)(2,1)}), bf16[2048,1408]{1,0:T(8,128)(2,1)}) %all-gather.6.cloned.1.call-update) | async-done | bytes 5767184 | tf_op jit(solution)/shard_map/all_gather | solution.py:98
  280.4 106.3 %all-gather.8.cloned.1.call-done = bf16[1408,2048]{1,0:T(8,128)(2,1)} async-done(((bf16[1408,512]{1,0:T(8,128)(2,1)}), bf16[1408,2048]{1,0:T(8,128)(2,1)}) %all-gather.8.cloned.1.call-update) | async-done | bytes 5767184 | tf_op jit(solution)/shard_map/all_gather | solution.py:99
  386.7 9.3 %convolution_convert_fusion.1 = bf16[256,2048]{1,0:T(8,128)(2,1)} fusion(bf16[1408,2048]{1,0:T(8,128)(2,1)} %all-gather.8.cloned.1.call-done, bf16[2048,1408]{1,0:T(8,128)(2,1)} %all-gather.6.cloned.1.call-done, f32[256,1408]{1,0:T(8,128)} %fusion.18, bf16[256,2048]{1,0:T(8,128)(2,1)S(1)} %get-tuple-element.132, f32[2048]{0:T(1024)S(1)} %copy-done.3, ...), kind=kOutput, calls=%fused_computation.21 | convolution fusion | flops 2957574144 | bytes 15082496 | tf_op jit(solution)/shard_map/dot_general | solution.py:104
  396.0 23.2 %reduce-scatter.2.cloned.1.call-done = bf16[64,2048]{1,0:T(8,128)(2,1)} async-done(((bf16[256,2048]{1,0:T(8,128)(2,1)}), bf16[64,2048]{1,0:T(8,128)(2,1)}) %reduce-scatter.2.cloned.1.call-update) | async-done | bytes 262160 | tf_op jit(solution)/shard_map/reduce_scatter | solution.py:103
  419.2 1.2 multiply_reduce_fusion
  420.4 1.8 multiply_convert_fusion
  (25 shorter events, 0.5 us)
Async XLA Ops:
  7.4 56.2 %copy-start = (bf16[256,2048]{1,0:T(8,128)(2,1)S(1)}, bf16[256,2048]{1,0:T(8,128)(2,1)}, u32[]{:S(2)}) copy-start(bf16[256,2048]{1,0:T(8,128)(2,1)} %param.17) | copy-start | bytes 3145732
  7.4 94.9 %all-reduce.2.cloned.1.call-start = ((), (), s32[]{:S(2)}) async-start(), calls=%async_computation.1 | async-start | bytes 2097152 | tf_op jit(solution)/shard_map/psum | solution.py:91
  56.5 3.3 copy-start.2
  63.5 38.7 %copy-start.1 = (bf16[256,2048]{1,0:T(8,128)(2,1)S(1)}, bf16[256,2048]{1,0:T(8,128)(2,1)}, u32[]{:S(2)}) copy-start(bf16[256,2048]{1,0:T(8,128)(2,1)} %param.12) | copy-start | bytes 3145732
  65.0 109.1 %copy-start.3 = (f32[2048]{0:T(1024)S(1)}, f32[2048]{0:T(1024)}, u32[]{:S(2)}) copy-start(f32[2048]{0:T(1024)} %param.18) | copy-start | bytes 24580
  65.0 109.1 %all-gather.4.cloned.1.call-start = ((), (), s32[]{:S(2)}) async-start(), calls=%async_computation.2 | async-start | bytes 7208960 | tf_op jit(solution)/shard_map/all_gather | solution.py:97
  65.6 214.8 %all-gather.6.cloned.1.call-start = ((), (), s32[]{:S(2)}) async-start(), calls=%async_computation.3 | async-start | bytes 7208960 | tf_op jit(solution)/shard_map/all_gather | solution.py:98
  66.2 320.5 %all-gather.8.cloned.1.call-start = ((), (), s32[]{:S(2)}) async-start(), calls=%async_computation.4 | async-start | bytes 7208960 | tf_op jit(solution)/shard_map/all_gather | solution.py:99
  66.8 352.4 %reduce-scatter.2.cloned.1.call-start = ((), (), s32[]{:S(2)}) async-start(), calls=%async_computation.5 | async-start | bytes 1310720 | tf_op jit(solution)/shard_map/reduce_scatter | solution.py:103
Sparse Core Ops, SparseCore 0:
  65.2 37.0 all-reduce.1
  396.1 23.0 reduce-scatter.1
Sparse Core Ops, SparseCore 1:
  67.1 107.0 all-gather.3
  175.6 104.8 all-gather.5
  281.9 104.8 all-gather.7
where the time goes:
time: 430 us
  waiting for transfers between devices  337 us (78%)
  blocking collectives  47 us (11%)
  matrix products  20 us (5%)
  between operations  15.1 us (4%)
  other arithmetic  6.94 us (2%)
    all_gather x1, waiting for transfers between devices, body(): down_whole = lax.all_gather(w_down, 'sp', axis=1, tiled=True)  106 us
    all_gather x1, waiting for transfers between devices, body(): up_whole = lax.all_gather(w_up, 'sp', axis=0, tiled=True)  101 us
    all_gather x1, waiting for transfers between devices, body(): gate_whole = lax.all_gather(w_gate, 'sp', axis=0, tiled=True)  70.1 us
    psum x1, waiting for transfers between devices, body(): lax.psum(jnp.dot(attended, w_out, preferred_element_type=jnp.float32).ast...  35.4 us
    reduce_scatter x1, waiting for transfers between devices, body(): lax.psum_scatter(jnp.dot(hidden, down_whole, preferred_element_type=jnp.f...  23.2 us
    all_gather x1, blocking collectives, attend(): lax.all_gather(keys.astype(jnp.float32), 'sp', axis=0, tiled=True)  17.4 us
    all_gather x1, blocking collectives, attend(): lax.all_gather(values.astype(jnp.float32), 'sp', axis=0, tiled=True)  16.3 us
    all_gather x1, blocking collectives, attend(): gate_piece = lax.all_gather(log_gates, 'sp', axis=0, tiled=True)  13.3 us
  transfers between devices with their start and end apart: 5, of which 5 were waited for; matrix products, arithmetic and copies ran while one was open for 2% of the time, Pallas kernels for 0%

commit v1 on v0

--- a/solution.py
+++ b/solution.py
@@ -88,8 +88,11 @@
     row_count = attended.shape[0]
     per_device = row_count // lax.axis_size("tp")
     my_first = lax.axis_index("tp") * per_device
-    projected = lax.psum(
-        jnp.dot(attended, w_out, preferred_element_type=jnp.float32).astype(jnp.bfloat16), "tp"
+    projected = jnp.sum(
+        lax.all_gather(
+            jnp.dot(attended, w_out, preferred_element_type=jnp.float32).astype(jnp.bfloat16), "tp"
+        ),
+        axis=0,
     ).astype(jnp.float32)
     mixed_all = (residual.astype(jnp.float32) + projected).astype(jnp.bfloat16)
     normed_all = normalize(mixed_all, norm_gain)

time: 430 us -> 463 us (1.077)
  waiting for transfers between devices: 337 us -> 369 us
    psum x1 -> x0, waiting for transfers between devices: 35.4 us -> none  [body(): lax.psum(jnp.dot(attended, w_out, preferred_element_type=jnp.float32).ast...]
    all_gather x1, waiting for transfers between devices: 70.1 us -> 103 us  [body(): gate_whole = lax.all_gather(w_gate, 'sp', axis=0, tiled=True)]
    all_gather x0 -> x1, waiting for transfers between devices: none -> 33 us  [body(): lax.all_gather(jnp.dot(attended, w_out, preferred_element_type=jnp.float3...]
    all_gather x1, waiting for transfers between devices: 101 us -> 106 us  [body(): up_whole = lax.all_gather(w_up, 'sp', axis=0, tiled=True)]
    all_gather x1, waiting for transfers between devices: 106 us -> 101 us  [body(): down_whole = lax.all_gather(w_down, 'sp', axis=1, tiled=True)]
where the time goes in v1:
time: 463 us
  waiting for transfers between devices  369 us (80%)
  blocking collectives  47 us (10%)
  matrix products  20.1 us (4%)
  between operations  13.2 us (3%)
  other arithmetic  10.1 us (2%)
    all_gather x1, waiting for transfers between devices, body(): up_whole = lax.all_gather(w_up, 'sp', axis=0, tiled=True)  106 us
    all_gather x1, waiting for transfers between devices, body(): gate_whole = lax.all_gather(w_gate, 'sp', axis=0, tiled=True)  103 us
    all_gather x1, waiting for transfers between devices, body(): down_whole = lax.all_gather(w_down, 'sp', axis=1, tiled=True)  101 us
    all_gather x1, waiting for transfers between devices, body(): lax.all_gather(jnp.dot(attended, w_out, preferred_element_type=jnp.float3...  33 us
    reduce_scatter x1, waiting for transfers between devices, body(): lax.psum_scatter(jnp.dot(hidden, down_whole, preferred_element_type=jnp.f...  23.2 us
    all_gather x1, blocking collectives, attend(): lax.all_gather(keys.astype(jnp.float32), 'sp', axis=0, tiled=True)  17.4 us
    all_gather x1, blocking collectives, attend(): lax.all_gather(values.astype(jnp.float32), 'sp', axis=0, tiled=True)  16.3 us
    all_gather x1, blocking collectives, attend(): gate_piece = lax.all_gather(log_gates, 'sp', axis=0, tiled=True)  13.3 us
  transfers between devices with their start and end apart: 5, of which 5 were waited for; matrix products, arithmetic and copies ran while one was open for 2% of the time, Pallas kernels for 0%

profile of v1, /device:TPU:0, one launch (start us, length us, event | category | flops | bytes accessed | tf_op | source)
XLA Modules:
  0.0 462.6 jit_solution(7669819110823955109)
XLA Ops:
  6.5 1.1 copy.12
  7.6 17.4 %all_gather.24 = bf16[1024,256]{0,1:T(8,128)(2,1)S(1)} all-gather(bf16[256,256]{0,1:T(8,128)(2,1)S(1)} %copy.12), channel_id=1, replica_groups=mesh['grp'=2,'sp'=4,'tp'=4] {'sp'}, dimensions={0}, use_global_device_ids=true | all-gather | bytes 655360 | tf_op jit(solution)/shard_map/all_gather | solution.py:29
  25.0 1.0 copy.13
  26.0 16.3 %all_gather.26 = bf16[1024,256]{0,1:T(8,128)(2,1)S(1)} all-gather(bf16[256,256]{0,1:T(8,128)(2,1)S(1)} %copy.13), channel_id=1, replica_groups=mesh['grp'=2,'sp'=4,'tp'=4] {'sp'}, dimensions={0}, use_global_device_ids=true | all-gather | bytes 655360 | tf_op jit(solution)/shard_map/all_gather | solution.py:32
  42.3 13.3 %all_gather.25 = f32[1024,4]{0,1:T(4,128)S(1)} all-gather(f32[256,4]{0,1:T(4,128)} %param.16), channel_id=1, replica_groups=mesh['grp'=2,'sp'=4,'tp'=4] {'sp'}, dimensions={0}, use_global_device_ids=true | all-gather | bytes 20480 | tf_op jit(solution)/shard_map/all_gather | solution.py:35
  55.7 7.1 %conditional.1 = ((f32[4,256]{1,0:T(4,128)S(1)}, f32[4,256,64]{1,2,0:T(8,128)S(1)})) conditional(s32[]{:T(128)} %convert_element_type.66, (f32[4,256]{1,0:T(4,128)S(1)}, f32[4,256,64]{1,2,0:T(8,128)S(1)}) %tuple.22, (s32[]{:T(128)}, s32[256]{0:T(256)S(1)}, bf16[256,256]{1,0:T(8,128)(2,1)}, bf16[1024,256]{0,1:T(8,128)(2,1)S(1)}, f32[4,256]{1,0:T(4,128)}, ...), branch_computations={%region_0.1_spmd, %region_1.0_spmd} | conditional | flops 288754944 | bytes 15727672 | solution.py:75
  56.0 1.0 copy.14
  57.0 2.1 fusion.2
  59.1 2.0 fusion.1
  61.1 1.6 fusion.6
  62.8 1.5 convolution_convert_fusion
  64.4 0.7 all-gather.6.cloned.1.call-update
  65.1 0.7 all-gather.10.cloned.1.call-update
  66.4 33.0 %all-gather.12.cloned.1.call-done = bf16[1024,2048]{1,0:T(8,128)(2,1)} async-done(((bf16[256,2048]{1,0:T(8,128)(2,1)}), bf16[1024,2048]{1,0:T(8,128)(2,1)}) %all-gather.12.cloned.1.call-update) | async-done | bytes 4194320 | tf_op jit(solution)/shard_map/all_gather | solution.py:92
  99.4 3.1 reduce_sum.41
  102.5 1.7 fusion.13
  104.2 103.5 %all-gather.6.cloned.1.call-done = bf16[2048,1408]{1,0:T(8,128)(2,1)} async-done(((bf16[512,1408]{1,0:T(8,128)(2,1)}), bf16[2048,1408]{1,0:T(8,128)(2,1)}) %all-gather.6.cloned.1.call-update) | async-done | bytes 5767184 | tf_op jit(solution)/shard_map/all_gather | solution.py:100
  207.7 5.7 %fusion.18 = f32[256,1408]{1,0:T(8,128)} fusion(bf16[2048,1408]{1,0:T(8,128)(2,1)} %all-gather.6.cloned.1.call-done, bf16[256,2048]{1,0:T(8,128)(2,1)S(1)} %get-tuple-element.132, f32[2048]{0:T(1024)S(1)} %copy-done.2, f32[256]{0:T(256)S(1)} %add_rsqrt_fusion), kind=kOutput, calls=%fused_computation.29 | convolution fusion | flops 1478492160 | bytes 8266752 | tf_op jit(solution)/shard_map/dot_general | solution.py:103
  213.3 100.9 %all-gather.10.cloned.1.call-done = bf16[1408,2048]{1,0:T(8,128)(2,1)} async-done(((bf16[1408,512]{1,0:T(8,128)(2,1)}), bf16[1408,2048]{1,0:T(8,128)(2,1)}) %all-gather.10.cloned.1.call-update) | async-done | bytes 5767184 | tf_op jit(solution)/shard_map/all_gather | solution.py:102
  314.2 106.4 %all-gather.8.cloned.1.call-done = bf16[2048,1408]{1,0:T(8,128)(2,1)} async-done(((bf16[512,1408]{1,0:T(8,128)(2,1)}), bf16[2048,1408]{1,0:T(8,128)(2,1)}) %all-gather.8.cloned.1.call-update) | async-done | bytes 5767184 | tf_op jit(solution)/shard_map/all_gather | solution.py:101
  420.6 9.3 %convolution_convert_fusion.1 = bf16[256,2048]{1,0:T(8,128)(2,1)} fusion(bf16[1408,2048]{1,0:T(8,128)(2,1)} %all-gather.10.cloned.1.call-done, bf16[2048,1408]{1,0:T(8,128)(2,1)} %all-gather.8.cloned.1.call-done, f32[256,1408]{1,0:T(8,128)} %fusion.18, bf16[256,2048]{1,0:T(8,128)(2,1)S(1)} %get-tuple-element.132, f32[2048]{0:T(1024)S(1)} %copy-done.2, ...), kind=kOutput, calls=%fused_computation.21 | convolution fusion | flops 2957574144 | bytes 15082496 | tf_op jit(solution)/shard_map/dot_general | solution.py:107
  429.9 23.2 %reduce-scatter.2.cloned.1.call-done = bf16[64,2048]{1,0:T(8,128)(2,1)} async-done(((bf16[256,2048]{1,0:T(8,128)(2,1)}), bf16[64,2048]{1,0:T(8,128)(2,1)}) %reduce-scatter.2.cloned.1.call-update) | async-done | bytes 262160 | tf_op jit(solution)/shard_map/reduce_scatter | solution.py:106
  453.1 1.2 multiply_reduce_fusion
  454.3 1.8 multiply_convert_fusion
  (24 shorter events, 1.0 us)
Async XLA Ops:
  6.5 56.3 %copy-start = (bf16[256,2048]{1,0:T(8,128)(2,1)S(1)}, bf16[256,2048]{1,0:T(8,128)(2,1)}, u32[]{:S(2)}) copy-start(bf16[256,2048]{1,0:T(8,128)(2,1)} %param.17) | copy-start | bytes 3145732
  6.5 92.8 %all-gather.12.cloned.1.call-start = ((), (), s32[]{:S(2)}) async-start(), calls=%async_computation.5 | async-start | bytes 5242880 | tf_op jit(solution)/shard_map/all_gather | solution.py:92
  55.7 3.3 copy-start.1
  64.3 143.4 %all-gather.6.cloned.1.call-start = ((), (), s32[]{:S(2)}) async-start(), calls=%async_computation.1 | async-start | bytes 7208960 | tf_op jit(solution)/shard_map/all_gather | solution.py:100
  65.1 249.2 %all-gather.10.cloned.1.call-start = ((), (), s32[]{:S(2)}) async-start(), calls=%async_computation.3 | async-start | bytes 7208960 | tf_op jit(solution)/shard_map/all_gather | solution.py:102
  65.8 354.8 %all-gather.8.cloned.1.call-start = ((), (), s32[]{:S(2)}) async-start(), calls=%async_computation.2 | async-start | bytes 7208960 | tf_op jit(solution)/shard_map/all_gather | solution.py:101
  66.4 386.7 %reduce-scatter.2.cloned.1.call-start = ((), (), s32[]{:S(2)}) async-start(), calls=%async_computation.4 | async-start | bytes 1310720 | tf_op jit(solution)/shard_map/reduce_scatter | solution.py:106
  99.4 108.3 %copy-start.2 = (f32[2048]{0:T(1024)S(1)}, f32[2048]{0:T(1024)}, u32[]{:S(2)}) copy-start(f32[2048]{0:T(1024)} %param.18) | copy-start | bytes 24580
Sparse Core Ops, SparseCore 0:
  64.4 34.8 all-gather.11
  100.9 106.6 all-gather.5
  209.2 104.9 all-gather.9
  315.6 104.9 all-gather.7
  430.0 23.0 reduce-scatter.1
